TPU v7x, 32 devices: a whole 2x2x4 slice. The times are simulated.
32 devices in a mesh: gr: 2 (over x), fs: 4 (over z), tp: 4 (over y, core).
Axes of the slice: x: 2, y: 2, z: 4, core: 2. Of those that a mesh axis runs over, the one named last changes fastest.
Arguments:
- prompt: bfloat16 [4096, 2048], P(('gr', 'fs')), may hold values from -6 to 6
- gain_first: float32 [2048], P(('gr', 'fs')), may hold values from 0.1 to 1.9
- gate_first: float32 [2048, 2816], P(('gr', 'fs'), 'tp'), may hold values from -0.125 to 0.125
- up_first: float32 [2048, 2816], P(('gr', 'fs'), 'tp'), may hold values from -0.125 to 0.125
- down_first: float32 [2816, 2048], P(('gr', 'fs'), 'tp'), may hold values from -0.109375 to 0.109375
- gain_second: float32 [2048], P(('gr', 'fs')), may hold values from 0.1 to 1.9
- gate_second: float32 [2048, 2816], P(('gr', 'fs'), 'tp'), may hold values from -0.125 to 0.125
- up_second: float32 [2048, 2816], P(('gr', 'fs'), 'tp'), may hold values from -0.125 to 0.125
- down_second: float32 [2816, 2048], P(('gr', 'fs'), 'tp'), may hold values from -0.109375 to 0.109375
Outputs:
- serve_gate_first: bfloat16 [2048, 2816], P(None, 'tp')
- serve_up_first: bfloat16 [2048, 2816], P(None, 'tp')
- serve_down_first: bfloat16 [2816, 2048], P('tp')
- serve_gate_second: bfloat16 [2048, 2816], P(None, 'tp')
- serve_up_second: bfloat16 [2048, 2816], P(None, 'tp')
- serve_down_second: bfloat16 [2816, 2048], P('tp')
- mixed: bfloat16 [4096, 2048], P(('gr', 'fs', 'tp'))
All inputs are finite; a program needn't handle non-finite values.
Results may differ from a plain program's by a relative error of at most 0.0085.
Values may be sent and summed in bfloat16 or wider, within the bound.
A program may use at most 128 MiB of HBM per device.

v0:
```python
import jax
import jax.numpy as jnp
from jax import lax
from jax.sharding import PartitionSpec as P


def normalize(rows):
    rows = rows.astype(jnp.float32)
    scale = lax.rsqrt(jnp.mean(rows * rows, axis=-1, keepdims=True) + 1e-06)
    return (rows * scale).astype(jnp.bfloat16)


def hidden_units(normed, w_gate, w_up):
    gate = jnp.dot(normed, w_gate, preferred_element_type=jnp.float32)
    upper = jnp.dot(normed, w_up, preferred_element_type=jnp.float32)
    return (jax.nn.silu(gate) * upper).astype(jnp.bfloat16)


def rounded_term(hidden, w_down):
    term = jnp.dot(hidden, w_down, preferred_element_type=jnp.float32).astype(jnp.bfloat16)
    return lax.optimization_barrier(term).astype(jnp.float32)


def shards(
    prompt,
    gain_first,
    gate_first,
    up_first,
    down_first,
    gain_second,
    gate_second,
    up_second,
    down_second,
):
    fold_gate_a = (gain_first[:, None] * gate_first).astype(jnp.bfloat16)
    fold_up_a = (gain_first[:, None] * up_first).astype(jnp.bfloat16)
    cast_down_a = down_first.astype(jnp.bfloat16)
    fold_gate_b = (gain_second[:, None] * gate_second).astype(jnp.bfloat16)
    fold_up_b = (gain_second[:, None] * up_second).astype(jnp.bfloat16)
    cast_down_b = down_second.astype(jnp.bfloat16)
    whole = (
        lax.all_gather(fold_gate_a, ("gr", "fs"), axis=0, tiled=True),
        lax.all_gather(fold_up_a, ("gr", "fs"), axis=0, tiled=True),
        lax.all_gather(cast_down_a, ("gr", "fs"), axis=0, tiled=True),
        lax.all_gather(fold_gate_b, ("gr", "fs"), axis=0, tiled=True),
        lax.all_gather(fold_up_b, ("gr", "fs"), axis=0, tiled=True),
        lax.all_gather(cast_down_b, ("gr", "fs"), axis=0, tiled=True),
    )
    gate_a, up_a, tall_a, gate_b, up_b, tall_b = whole
    down_a, down_b = (
        lax.all_to_all(tall_a, "tp", split_axis=0, concat_axis=1, tiled=True),
        lax.all_to_all(tall_b, "tp", split_axis=0, concat_axis=1, tiled=True),
    )
    hidden_a = hidden_units(normalize(prompt), gate_a, up_a)
    branch_a = lax.psum(rounded_term(hidden_a, down_a).astype(jnp.bfloat16), "tp").astype(
        jnp.float32
    )
    stream = prompt.astype(jnp.float32) + 0.5 * branch_a
    hidden_b = hidden_units(normalize(stream), gate_b, up_b)
    owned = hidden_b.shape[0] // lax.axis_size("tp")
    branch_b = lax.psum_scatter(
        rounded_term(hidden_b, down_b).astype(jnp.bfloat16), "tp", scatter_dimension=0, tiled=True
    ).astype(jnp.float32)
    own_stream = lax.dynamic_slice_in_dim(stream, lax.axis_index("tp") * owned, owned, 0)
    mixed = (own_stream + 0.5 * branch_b).astype(jnp.bfloat16)
    return (gate_a, up_a, down_a, gate_b, up_b, down_b, mixed)


def solution(mesh):
    return jax.shard_map(
        shards,
        mesh=mesh,
        in_specs=(
            P(("gr", "fs"), None),
            P(("gr", "fs")),
            P(("gr", "fs"), "tp"),
            P(("gr", "fs"), "tp"),
            P(("gr", "fs"), "tp"),
            P(("gr", "fs")),
            P(("gr", "fs"), "tp"),
            P(("gr", "fs"), "tp"),
            P(("gr", "fs"), "tp"),
        ),
        out_specs=(
            P(None, "tp"),
            P(None, "tp"),
            P("tp", None),
            P(None, "tp"),
            P(None, "tp"),
            P("tp", None),
            P(("gr", "fs", "tp"), None),
        ),
        check_vma=False,
    )
```

profile of v0, /device:TPU:25, one launch (start us, length us, event | category | flops | bytes accessed | tf_op | source)
XLA Modules:
  0.0 497.4 jit_solution(5870135951436558811)
XLA Ops:
  7.2 0.0 copy-start.5
  7.2 0.0 all-gather.11.cloned.1.call-start
  7.2 1.9 convert_element_type.55
  9.2 0.0 all-gather.11.cloned.1.call-update
  9.2 0.0 all-gather.7.cloned.1.call-start
  9.2 2.3 multiply_convert_fusion.3
  11.6 0.0 all-gather.7.cloned.1.call-update
  11.6 0.0 all-gather.9.cloned.1.call-start
  11.6 0.7 all-gather.9.cloned.1.call-update
  12.3 0.0 all-gather.17.cloned.1.call-start
  12.4 0.8 convert_element_type.58
  13.2 0.0 all-gather.17.cloned.1.call-update
  13.2 53.7 %all-gather.11.cloned.1.call-done = bf16[2816,512]{1,0:T(8,128)(2,1)} async-done(((bf16[352,512]{1,0:T(8,128)(2,1)}), bf16[2816,512]{1,0:T(8,128)(2,1)}) %all-gather.11.cloned.1.call-update) | async-done | bytes 2883600 | tf_op jit(solution)/shard_map/all_gather | solution.py:44
  66.9 5.0 %all-to-all-start = ((bf16[4,704,512]{2,1,0:T(8,128)(2,1)}), bf16[4,704,512]{2,1,0:T(8,128)(2,1)S(1)}, u32[]{:S(2)}, u32[]{:S(2)}) async-start(bf16[4,704,512]{2,1,0:T(8,128)(2,1)} %bitcast.21), calls=%async_computation | async-start | bytes 5767168 | tf_op jit(solution)/shard_map/all_to_all | solution.py:51
  71.9 0.0 all-reduce.2.cloned.1.call-start
  71.9 2.1 fusion
  74.0 54.0 %all-gather.7.cloned.1.call-done = bf16[2048,704]{0,1:T(8,128)(2,1)} async-done(((bf16[256,704]{0,1:T(8,128)(2,1)}), bf16[2048,704]{0,1:T(8,128)(2,1)}) %all-gather.7.cloned.1.call-update) | async-done | bytes 2883600 | tf_op jit(solution)/shard_map/all_gather | solution.py:42
  127.9 5.3 %fusion.5 = f32[512,704]{0,1:T(8,128)} fusion(bf16[2048,704]{0,1:T(8,128)(2,1)} %all-gather.7.cloned.1.call-done, bf16[512,2048]{1,0:T(8,128)(2,1)} %param.9, f32[512]{0:T(512)S(1)} %add_rsqrt_fusion.1), kind=kOutput, calls=%fused_computation.14 | convolution fusion | flops 1479540736 | bytes 6424576 | tf_op jit(solution)/shard_map/dot_general | solution.py:14
  133.3 0.0 all-to-all-done
  133.3 2.0 copy.20
  135.3 53.0 %all-gather.9.cloned.1.call-done = bf16[2048,704]{0,1:T(8,128)(2,1)} async-done(((bf16[256,704]{0,1:T(8,128)(2,1)}), bf16[2048,704]{0,1:T(8,128)(2,1)}) %all-gather.9.cloned.1.call-update) | async-done | bytes 2883600 | tf_op jit(solution)/shard_map/all_gather | solution.py:43
  188.3 8.7 %convolution_convert_fusion.1 = bf16[512,2048]{1,0:T(8,128)(2,1)} fusion(bf16[704,2048]{1,0:T(8,128)(2,1)} %bitcast.16, bf16[2048,704]{0,1:T(8,128)(2,1)} %all-gather.9.cloned.1.call-done, f32[512,704]{0,1:T(8,128)} %fusion.5, bf16[512,2048]{1,0:T(8,128)(2,1)} %param.9, f32[512]{0:T(512)S(1)} %add_rsqrt_fusion.1), kind=kOutput, calls=%fused_computation.8 | convolution fusion | flops 2959147008 | bytes 11405312 | tf_op jit(solution)/shard_map/dot_general | solution.py:20
  197.0 0.0 all-reduce.2.cloned.1.call-update
  197.0 0.0 all-gather.13.cloned.1.call-start
  197.1 1.0 multiply_convert_fusion.1
  198.1 0.0 all-gather.13.cloned.1.call-update
  198.1 0.0 all-gather.15.cloned.1.call-start
  198.2 0.7 all-gather.15.cloned.1.call-update
  198.9 0.0 reduce-scatter.2.cloned.1.call-start
  198.9 47.2 %all-gather.17.cloned.1.call-done = bf16[2816,512]{1,0:T(8,128)(2,1)} async-done(((bf16[352,512]{1,0:T(8,128)(2,1)}), bf16[2816,512]{1,0:T(8,128)(2,1)}) %all-gather.17.cloned.1.call-update) | async-done | bytes 2883600 | tf_op jit(solution)/shard_map/all_gather | solution.py:47
  246.1 55.7 %all_to_all.38 = bf16[4,704,512]{2,1,0:T(8,128)(2,1)S(1)} all-to-all(bf16[4,704,512]{2,1,0:T(8,128)(2,1)} %bitcast.18), channel_id=1, replica_groups=mesh['gr'=2,'fs'=4,'tp'=4] {'tp'}, dimensions={0} | all-to-all | bytes 5767168 | tf_op jit(solution)/shard_map/all_to_all | solution.py:52
  301.8 2.0 copy.21
  303.8 14.8 %all-reduce.2.cloned.1.call-done = bf16[512,2048]{1,0:T(8,128)(2,1)} async-done(((bf16[512,2048]{1,0:T(8,128)(2,1)}), bf16[512,2048]{1,0:T(8,128)(2,1)}) %all-reduce.2.cloned.1.call-update) | async-done | bytes 2097168 | tf_op jit(solution)/shard_map/psum | solution.py:55
  318.6 4.3 convert_add_fusion
  323.0 55.2 %all-gather.13.cloned.1.call-done = bf16[2048,704]{0,1:T(8,128)(2,1)} async-done(((bf16[256,704]{0,1:T(8,128)(2,1)}), bf16[2048,704]{0,1:T(8,128)(2,1)}) %all-gather.13.cloned.1.call-update) | async-done | bytes 2883600 | tf_op jit(solution)/shard_map/all_gather | solution.py:45
  378.2 4.2 fusion.12
  382.5 56.1 %all-gather.15.cloned.1.call-done = bf16[2048,704]{0,1:T(8,128)(2,1)} async-done(((bf16[256,704]{0,1:T(8,128)(2,1)}), bf16[2048,704]{0,1:T(8,128)(2,1)}) %all-gather.15.cloned.1.call-update) | async-done | bytes 2883600 | tf_op jit(solution)/shard_map/all_gather | solution.py:46
  438.6 8.3 %convolution_convert_fusion = bf16[512,2048]{1,0:T(8,128)(2,1)} fusion(bf16[704,2048]{1,0:T(8,128)(2,1)} %bitcast.19, bf16[2048,704]{0,1:T(8,128)(2,1)} %all-gather.15.cloned.1.call-done, f32[512,704]{0,1:T(8,128)S(1)} %fusion.12, f32[512]{0:T(512)S(1)} %add_rsqrt_fusion, bf16[512,2048]{1,0:T(8,128)(2,1)S(1)} %copy-done, ...), kind=kOutput, calls=%fused_computation.7 | convolution fusion | flops 2962292736 | bytes 13502464 | tf_op jit(solution)/shard_map/dot_general | solution.py:20
  446.9 0.0 reduce-scatter.2.cloned.1.call-update
  446.9 31.2 %reduce-scatter.2.cloned.1.call-done = bf16[128,2048]{1,0:T(8,128)(2,1)} async-done(((bf16[512,2048]{1,0:T(8,128)(2,1)}), bf16[128,2048]{1,0:T(8,128)(2,1)}) %reduce-scatter.2.cloned.1.call-update) | async-done | bytes 524304 | tf_op jit(solution)/shard_map/reduce_scatter | solution.py:61
  478.1 2.3 add_convert_fusion
  480.4 1.6 copy.27
  482.0 1.3 copy-done.2
  483.2 1.6 copy.28
  484.8 1.3 copy-done.3
  486.1 1.6 copy.29
  487.7 1.3 copy-done.4
  489.0 1.6 copy.30
  (16 shorter events, 0.0 us)
Async XLA Ops:
  7.2 5.2 %copy-start.5 = (f32[352,512]{1,0:T(8,128)S(1)}, f32[352,512]{1,0:T(8,128)}, u32[]{:S(2)}) copy-start(f32[352,512]{1,0:T(8,128)} %param.17) | copy-start | bytes 2162692
  7.2 59.7 %all-gather.11.cloned.1.call-start = ((), (), s32[]{:S(2)}) async-start(), calls=%async_computation.5 | async-start | bytes 3244032 | tf_op jit(solution)/shard_map/all_gather | solution.py:44
  9.2 118.7 %all-gather.7.cloned.1.call-start = ((), (), s32[]{:S(2)}) async-start(), calls=%async_computation.3 | async-start | bytes 3244032 | tf_op jit(solution)/shard_map/all_gather | solution.py:42
  11.6 176.7 %all-gather.9.cloned.1.call-start = ((), (), s32[]{:S(2)}) async-start(), calls=%async_computation.4 | async-start | bytes 3244032 | tf_op jit(solution)/shard_map/all_gather | solution.py:43
  12.3 233.8 %all-gather.17.cloned.1.call-start = ((), (), s32[]{:S(2)}) async-start(), calls=%async_computation.8 | async-start | bytes 3244032 | tf_op jit(solution)/shard_map/all_gather | solution.py:47
  66.9 66.4 %all-to-all-start = ((bf16[4,704,512]{2,1,0:T(8,128)(2,1)}), bf16[4,704,512]{2,1,0:T(8,128)(2,1)S(1)}, u32[]{:S(2)}, u32[]{:S(2)}) async-start(bf16[4,704,512]{2,1,0:T(8,128)(2,1)} %bitcast.21), calls=%async_computation | async-start | bytes 5767168 | tf_op jit(solution)/shard_map/all_to_all | solution.py:51
  71.9 246.7 %all-reduce.2.cloned.1.call-start = ((), (), s32[]{:S(2)}) async-start(), calls=%async_computation.9 | async-start | bytes 4194304 | tf_op jit(solution)/shard_map/psum | solution.py:55
  188.3 8.8 %copy-start.6 = (f32[256,704]{0,1:T(8,128)S(1)}, f32[256,704]{0,1:T(8,128)}, u32[]{:S(2)}) copy-start(f32[256,704]{0,1:T(8,128)} %param.16) | copy-start | bytes 2162692
  188.3 8.8 %copy-start.7 = (f32[256,704]{0,1:T(8,128)S(1)}, f32[256,704]{0,1:T(8,128)}, u32[]{:S(2)}) copy-start(f32[256,704]{0,1:T(8,128)} %param.15) | copy-start | bytes 2162692
  188.3 8.8 %copy-start.8 = (f32[256]{0:T(256)S(1)}, f32[256]{0:T(256)}, u32[]{:S(2)}) copy-start(f32[256]{0:T(256)} %param.14) | copy-start | bytes 3076
  197.0 181.2 %all-gather.13.cloned.1.call-start = ((), (), s32[]{:S(2)}) async-start(), calls=%async_computation.6 | async-start | bytes 3244032 | tf_op jit(solution)/shard_map/all_gather | solution.py:45
  198.1 240.5 %all-gather.15.cloned.1.call-start = ((), (), s32[]{:S(2)}) async-start(), calls=%async_computation.7 | async-start | bytes 3244032 | tf_op jit(solution)/shard_map/all_gather | solution.py:46
  198.9 279.2 %reduce-scatter.2.cloned.1.call-start = ((), (), s32[]{:S(2)}) async-start(), calls=%async_computation.10 | async-start | bytes 2621440 | tf_op jit(solution)/shard_map/reduce_scatter | solution.py:61
  301.8 16.8 %copy-start = (bf16[512,2048]{1,0:T(8,128)(2,1)S(1)}, bf16[512,2048]{1,0:T(8,128)(2,1)}, u32[]{:S(2)}) copy-start(bf16[512,2048]{1,0:T(8,128)(2,1)} %param.9) | copy-start | bytes 6291460
  446.9 33.5 %copy-start.1 = (bf16[2048,704]{0,1:T(8,128)(2,1)S(1)}, bf16[2048,704]{0,1:T(8,128)(2,1)}, u32[]{:S(2)}) copy-start(bf16[2048,704]{0,1:T(8,128)(2,1)} %all-gather.7.cloned.1.call-done) | copy-start | bytes 8650756
  480.4 2.9 copy-start.2
  483.2 2.9 copy-start.3
  486.1 2.9 copy-start.4
Sparse Core Ops, SparseCore 0:
  10.7 56.1 all-gather.10
  69.4 58.4 all-gather.6
  130.5 57.7 all-gather.8
  190.8 55.2 all-gather.16
  248.9 69.7 all-reduce.1
  321.1 57.1 all-gather.12
  380.8 57.7 all-gather.14
  447.0 30.9 reduce-scatter.1
where the time goes:
time: 500 us; the launch traced here: 497 us
  waiting for transfers between devices  367 us (73%)
  blocking collectives  55.7 us (11%)
  matrix products  26.5 us (5%)
  other arithmetic  14.7 us (3%)
  local copies, waits for them, and re-layouts  14.2 us (3%)
  between operations  14.2 us (3%)
  starting transfers between devices  5.32 us (1%)
    all_gather x1, waiting for transfers between devices, shards(): lax.all_gather(fold_up_b, ('gr', 'fs'), axis=0, tiled=True)  56.1 us
    all_to_all x1, blocking collectives, shards(): lax.all_to_all(tall_b, 'tp', split_axis=0, concat_axis=1, tiled=True)  55.7 us
    all_gather x1, waiting for transfers between devices, shards(): lax.all_gather(fold_gate_b, ('gr', 'fs'), axis=0, tiled=True)  55.2 us
    all_gather x1, waiting for transfers between devices, shards(): lax.all_gather(fold_gate_a, ('gr', 'fs'), axis=0, tiled=True)  54 us
    all_gather x1, waiting for transfers between devices, shards(): lax.all_gather(cast_down_a, ('gr', 'fs'), axis=0, tiled=True)  53.7 us
    all_gather x1, waiting for transfers between devices, shards(): lax.all_gather(fold_up_a, ('gr', 'fs'), axis=0, tiled=True)  53 us
    all_gather x1, waiting for transfers between devices, shards(): lax.all_gather(cast_down_b, ('gr', 'fs'), axis=0, tiled=True)  47.2 us
    reduce_scatter x1, waiting for transfers between devices, shards(): lax.psum_scatter(rounded_term(hidden_b, down_b).astype(jnp.bfloat16), 'tp...  31.2 us
  transfers between devices with their start and end apart: 9, of which 8 were waited for; matrix products, arithmetic and copies ran while one was open for 7% of the time, Pallas kernels for 0%

commit v1 on v0

v1 whole, which is shorter than its diff:
```python
import functools

import jax
import jax.numpy as jnp
from jax import lax
from jax.experimental import pallas as pl
from jax.experimental.pallas import tpu as pltpu
from jax.sharding import PartitionSpec as P

MESH = pl.DeviceIdType.MESH


def gather_kernel(
    n_gr,
    n_fs,
    n_tp,
    gain_ref,
    gate_ref,
    up_ref,
    down_ref,
    gate_out,
    up_out,
    down_out,
    down_own,
    line_send,
    line_recv,
    pair_send,
    pair_recv,
    part_send,
    part_recv,
):
    g, f, t = lax.axis_index("gr"), lax.axis_index("fs"), lax.axis_index("tp")
    per = n_gr * n_fs // n_tp
    cols = down_ref.shape[1]
    first = lax.rem(t * per, n_fs)
    home = (t * per) // n_fs
    row = g * n_fs + f
    owner = row // per
    slot = lax.rem(row, per)

    width = gate_ref.shape[1]

    def place(ref, origin):
        if len(ref.shape) == 3:
            return ref.at[origin]
        return ref.at[:, pl.ds(pl.multiple_of(origin * width, 128), width)]

    gain = gain_ref[...]
    place(gate_out, row)[...] = (gain * gate_ref[...]).astype(jnp.bfloat16)
    place(up_out, row)[...] = (gain * up_ref[...]).astype(jnp.bfloat16)
    down_own[...] = down_ref[...].astype(jnp.bfloat16)

    @pl.when(owner == t)
    def _():
        down_out[slot, :, pl.ds(pl.multiple_of(t * cols, 128), cols)] = down_ref[...].astype(
            jnp.bfloat16
        )

    barrier = pltpu.get_barrier_semaphore()
    for dg in range(n_gr):
        for dt in range(n_tp):
            if dg or dt:
                pl.semaphore_signal(
                    barrier,
                    inc=1,
                    device_id=(lax.rem(g + dg, n_gr), f, lax.rem(t + dt, n_tp)),
                    device_id_type=MESH,
                )

    for near in (lax.rem(f + 1, n_fs), lax.rem(f + n_fs - 1, n_fs)):
        pl.semaphore_signal(barrier, inc=1, device_id=(g, near, t), device_id_type=MESH)
    pl.semaphore_wait(barrier, n_gr * n_tp + 1)

    outs = (gate_out, up_out)

    def held(o):
        return jnp.logical_and(o >= first, o < first + per)

    def block(m, o):
        if m < 2:
            return place(outs[m], g * n_fs + o)
        return down_out.at[o - first]

    def line(m, way, s):
        step = 1 if way == 0 else -1
        o = f - step * (s - 1)
        return pltpu.make_async_remote_copy(
            src_ref=block(m, o),
            dst_ref=block(m, o),
            send_sem=line_send.at[m, way, s],
            recv_sem=line_recv.at[m, way, s],
            device_id=(g, f + step, t),
            device_id_type=MESH,
        )

    def sends(m, way, s):
        step = 1 if way == 0 else -1
        o = f - step * (s - 1)
        fine = (f < n_fs - 1, o >= 0) if way == 0 else (f > 0, o <= n_fs - 1)
        ok = jnp.logical_and(*fine)
        return jnp.logical_and(ok, held(o)) if m == 2 else ok

    def gets(m, way, s):
        o = f - s if way == 0 else f + s
        ok = o >= 0 if way == 0 else o <= n_fs - 1
        return jnp.logical_and(ok, held(o)) if m == 2 else ok

    def landed(m, way, s):
        o = f - s if way == 0 else f + s
        return pltpu.make_async_remote_copy(
            src_ref=block(m, o),
            dst_ref=block(m, o),
            send_sem=line_send.at[m, way, s],
            recv_sem=line_recv.at[m, way, s],
            device_id=(g, f, t),
            device_id_type=MESH,
        )

    def pair(m, dg, o):
        return pltpu.make_async_remote_copy(
            src_ref=place(outs[m], g * n_fs + o),
            dst_ref=place(outs[m], g * n_fs + o),
            send_sem=pair_send.at[m, dg, o],
            recv_sem=pair_recv.at[m, dg, o],
            device_id=(lax.rem(g + dg, n_gr), f, t),
            device_id_type=MESH,
        )

    def pair_landed(m, dg, o):
        src = lax.rem(g - dg + n_gr, n_gr)
        return pltpu.make_async_remote_copy(
            src_ref=place(outs[m], src * n_fs + o),
            dst_ref=place(outs[m], src * n_fs + o),
            send_sem=pair_send.at[m, dg, o],
            recv_sem=pair_recv.at[m, dg, o],
            device_id=(src, f, t),
            device_id_type=MESH,
        )

    def part(dg):
        to = lax.rem(g + dg, n_gr)
        return pltpu.make_async_remote_copy(
            src_ref=down_own,
            dst_ref=down_out.at[slot, :, pl.ds(pl.multiple_of(t * cols, 128), cols)],
            send_sem=part_send.at[dg],
            recv_sem=part_recv.at[t],
            device_id=(to, f, owner),
            device_id_type=MESH,
        )

    def part_landed(src):
        return pltpu.make_async_remote_copy(
            src_ref=down_own,
            dst_ref=down_out.at[f - first, :, pl.ds(src * cols, cols)],
            send_sem=part_send.at[0],
            recv_sem=part_recv.at[src],
            device_id=(home, f, src),
            device_id_type=MESH,
        )

    for m in range(2):
        for way in range(2):

            @pl.when(sends(m, way, 1))
            def _(m=m, way=way):
                line(m, way, 1).start()

        for dg in range(1, n_gr):
            pair(m, dg, f).start()
    for dg in range(n_gr):
        if dg == 0:

            @pl.when(owner != t)
            def _():
                part(0).start()

        else:
            part(dg).start()

    @pl.when(held(f))
    def _():
        for src in range(n_tp):

            @pl.when(jnp.logical_or(home != g, t != src))
            def _(src=src):
                part_landed(src).wait_recv()

    for way in range(2):

        @pl.when(sends(2, way, 1))
        def _(way=way):
            line(2, way, 1).start()

    for s in range(1, n_fs):
        for m in range(3):
            for way in range(2):

                @pl.when(gets(m, way, s))
                def _(m=m, way=way, s=s):
                    landed(m, way, s).wait_recv()
                    if s < n_fs - 1:

                        @pl.when(sends(m, way, s + 1))
                        def _():
                            line(m, way, s + 1).start()

                    if m < 2:
                        o = f - s if way == 0 else f + s
                        for dg in range(1, n_gr):
                            pair(m, dg, o).start()

    for m in range(2):
        for dg in range(1, n_gr):
            for o in range(n_fs):
                pair_landed(m, dg, o).wait_recv()
                pair(m, dg, o).wait_send()
    for m in range(3):
        for way in range(2):
            for s in range(1, n_fs):

                @pl.when(sends(m, way, s))
                def _(m=m, way=way, s=s):
                    line(m, way, s).wait_send()

    for dg in range(n_gr):
        if dg == 0:

            @pl.when(owner != t)
            def _():
                part(0).wait_send()

        else:
            part(dg).wait_send()


def gather(sizes, call, gain, gate, up, down):
    n_gr, n_fs, n_tp = sizes
    per = n_gr * n_fs // n_tp
    rows, width = gate.shape
    wide = rows % 128 == 0
    whole = (width, n_gr * n_fs * rows) if wide else (n_gr * n_fs, width, rows)
    tall, cols = down.shape
    vmem = pl.BlockSpec(memory_space=pltpu.VMEM)
    dma = pltpu.SemaphoreType.DMA
    gate_all, up_all, down_all = pl.pallas_call(
        functools.partial(gather_kernel, n_gr, n_fs, n_tp),
        out_shape=(
            jax.ShapeDtypeStruct(whole, jnp.bfloat16),
            jax.ShapeDtypeStruct(whole, jnp.bfloat16),
            jax.ShapeDtypeStruct((per, tall, n_tp * cols), jnp.bfloat16),
        ),
        in_specs=[vmem] * 4,
        out_specs=(vmem,) * 3,
        scratch_shapes=[
            pltpu.VMEM((tall, cols), jnp.bfloat16),
            dma((3, 2, n_fs)),
            dma((3, 2, n_fs)),
            dma((2, n_gr, n_fs)),
            dma((2, n_gr, n_fs)),
            dma((n_gr,)),
            dma((n_tp,)),
        ],
        compiler_params=pltpu.CompilerParams(
            collective_id=call, has_side_effects=True, vmem_limit_bytes=32 * 2**20
        ),
        cost_estimate=pl.CostEstimate(
            flops=10**10, bytes_accessed=16 * 2**20, transcendentals=0
        ),
    )(gain[None, :], gate.T, up.T, down)

    def upright(a):
        return a.T if wide else a.transpose(0, 2, 1).reshape(n_gr * n_fs * rows, width)

    return (
        upright(gate_all),
        upright(up_all),
        down_all.reshape(per * tall, n_tp * cols),
    )


def normalize(rows):
    rows = rows.astype(jnp.float32)
    scale = lax.rsqrt(jnp.mean(rows * rows, axis=-1, keepdims=True) + 1e-06)
    return (rows * scale).astype(jnp.bfloat16)


def hidden_units(normed, w_gate, w_up):
    gate = jnp.dot(normed, w_gate, preferred_element_type=jnp.float32)
    upper = jnp.dot(normed, w_up, preferred_element_type=jnp.float32)
    return (jax.nn.silu(gate) * upper).astype(jnp.bfloat16)


def rounded_term(hidden, w_down):
    return jnp.dot(hidden, w_down, preferred_element_type=jnp.float32).astype(jnp.bfloat16)


def shards(
    sizes,
    prompt,
    gain_first,
    gate_first,
    up_first,
    down_first,
    gain_second,
    gate_second,
    up_second,
    down_second,
):
    gate_a, up_a, down_a = gather(sizes, 0, gain_first, gate_first, up_first, down_first)
    hidden_a = hidden_units(normalize(prompt), gate_a, up_a)
    term_a = rounded_term(hidden_a, down_a)
    term_a, gain_second = lax.optimization_barrier((term_a, gain_second))
    branch_a = lax.psum(term_a, "tp").astype(jnp.float32)
    gate_b, up_b, down_b = gather(sizes, 1, gain_second, gate_second, up_second, down_second)
    stream = prompt.astype(jnp.float32) + 0.5 * branch_a
    hidden_b = hidden_units(normalize(stream), gate_b, up_b)
    owned = hidden_b.shape[0] // lax.axis_size("tp")
    branch_b = lax.psum_scatter(
        rounded_term(hidden_b, down_b), "tp", scatter_dimension=0, tiled=True
    ).astype(jnp.float32)
    own_stream = lax.dynamic_slice_in_dim(stream, lax.axis_index("tp") * owned, owned, 0)
    mixed = (own_stream + 0.5 * branch_b).astype(jnp.bfloat16)
    return (gate_a, up_a, down_a, gate_b, up_b, down_b, mixed)


def solution(mesh):
    sizes = (mesh.shape["gr"], mesh.shape["fs"], mesh.shape["tp"])
    return jax.shard_map(
        functools.partial(shards, sizes),
        mesh=mesh,
        in_specs=(
            P(("gr", "fs"), None),
            P(("gr", "fs")),
            P(("gr", "fs"), "tp"),
            P(("gr", "fs"), "tp"),
            P(("gr", "fs"), "tp"),
            P(("gr", "fs")),
            P(("gr", "fs"), "tp"),
            P(("gr", "fs"), "tp"),
            P(("gr", "fs"), "tp"),
        ),
        out_specs=(
            P(None, "tp"),
            P(None, "tp"),
            P("tp", None),
            P(None, "tp"),
            P(None, "tp"),
            P("tp", None),
            P(("gr", "fs", "tp"), None),
        ),
        check_vma=False,
    )
```

time: 500 us -> 305 us (0.61)
  waiting for transfers between devices: 367 us -> 51.9 us
  Pallas kernels: 0 us -> 177 us
  blocking collectives: 55.7 us -> 0 us
  local copies, waits for them, and re-layouts: 14.2 us -> 27.8 us
  starting transfers between devices: 5.32 us -> 0.08 us
  other arithmetic: 14.7 us -> 9.54 us
    all_gather x6 -> x0, waiting for transfers between devices: 319 us -> none  [the longest x1 56.1 us: shards(): lax.all_gather(fold_up_b, ('gr', 'fs'), axis=0, tiled=True)]
    pallas_call x0 -> x2, Pallas kernels: none -> 177 us  [gather(): pl.pallas_call(functools.partial(gather_kernel, n_gr, n_fs, n_tp), out_sh...]
    all_to_all x1 -> x0, blocking collectives: 55.7 us -> none  [shards(): lax.all_to_all(tall_b, 'tp', split_axis=0, concat_axis=1, tiled=True)]
    reduce_scatter x1, waiting for transfers between devices: 31.2 us -> 51.9 us  [shards(): lax.psum_scatter(rounded_term(hidden_b, down_b), 'tp', scatter_dimension=...]
    unnamed x22 -> x48, local copies, waits for them, and re-layouts: 10.2 us -> 27.8 us
    psum x1, waiting for transfers between devices: 14.8 us -> 0.01 us  [shards(): branch_a = lax.psum(term_a, 'tp').astype(jnp.float32)]
    convert_element_type x4 -> x0, other arithmetic: 6.01 us -> none  [the longest x1 2.31 us: shards(): fold_up_a = (gain_first[:, None] * up_first).astype(jnp.bfloat16)]
    all_to_all x1 -> x0, starting transfers between devices: 5.04 us -> none  [shards(): lax.all_to_all(tall_a, 'tp', split_axis=0, concat_axis=1, tiled=True)]
  transfers between devices with their start and end apart: 9 -> 2, of which waited for: 8 -> 1; matrix products, arithmetic and copies ran while one was open for 7% -> 0% of each run, Pallas kernels for 0% -> 32%
where the time goes in v1:
time: 305 us; the launch traced here: 303 us
  Pallas kernels  177 us (58%)
  waiting for transfers between devices  51.9 us (17%)
  local copies, waits for them, and re-layouts  27.8 us (9%)
  matrix products  22.8 us (7%)
  between operations  14.2 us (5%)
  other arithmetic  9.54 us (3%)
    pallas_call x2, Pallas kernels, gather(): pl.pallas_call(functools.partial(gather_kernel, n_gr, n_fs, n_tp), out_sh...  177 us
    reduce_scatter x1, waiting for transfers between devices, shards(): lax.psum_scatter(rounded_term(hidden_b, down_b), 'tp', scatter_dimension=...  51.9 us
    unnamed x48, local copies, waits for them, and re-layouts  27.8 us
    dot_general x2, matrix products, rounded_term(): jnp.dot(hidden, w_down, preferred_element_type=jnp.float32)  17 us
  transfers between devices with their start and end apart: 2, of which 1 were waited for; matrix products, arithmetic and copies ran while one was open for 0% of the time, Pallas kernels for 32%

profile of v1, /device:TPU:25, one launch (start us, length us, event | category | flops | bytes accessed | tf_op | source)
XLA Modules:
  0.0 303.0 jit_solution(1822066774879081391)
XLA Ops:
  7.2 0.0 all-reduce.2.cloned.1.call-start
  7.2 2.1 fusion
  9.3 0.0 copy-start.10
  9.3 1.1 copy-done.10
  10.4 0.0 copy-start.11
  10.4 1.1 copy-done.11
  11.5 0.0 copy-start.12
  11.5 1.1 copy-done.12
  12.6 0.7 copy-done.16
  13.3 79.8 %shard_map.144 = (bf16[704,2048]{1,0:T(8,128)(2,1)S(1)}, bf16[704,2048]{1,0:T(8,128)(2,1)S(1)}, bf16[2,352,2048]{2,1,0:T(8,128)(2,1)S(1)}) custom-call(f32[1,256]{1,0:T(1,128)S(1)} %bitcast.30, f32[704,256]{1,0:T(8,128)S(1)} %bitcast.26, f32[704,256]{1,0:T(8,128)S(1)} %bitcast.27, f32[352,512]{1,0:T(8,128)S(1)} %copy-done.12), custom_call_target="tpu_custom_call" | custom-call | flops 10000000000 | bytes 16777216 | tf_op jit(solution)/shard_map/pallas_call | solution.py:245
  93.1 0.0 copy-start
  93.1 0.0 copy-start.2
  93.2 0.0 copy-done.18
  93.2 3.0 fusion.5
  96.1 0.0 copy-done
  96.1 0.0 copy-done.2
  96.1 7.7 %convolution_convert_fusion.1 = bf16[512,2048]{1,0:T(8,128)(2,1)} fusion(bf16[704,2048]{1,0:T(8,128)(2,1)S(1)} %bitcast.18, bf16[704,2048]{1,0:T(8,128)(2,1)} %copy-done, f32[512,704]{0,1:T(8,128)} %fusion.5, bf16[512,2048]{1,0:T(8,128)(2,1)} %param.9, f32[512]{0:T(512)S(1)} %add_rsqrt_fusion.1), kind=kOutput, calls=%fused_computation.8 | convolution fusion | flops 2959147008 | bytes 11405312 | tf_op jit(solution)/shard_map/dot_general | solution.py:294
  103.9 0.0 all-reduce.2.cloned.1.call-update
  103.9 0.0 reduce-scatter.2.cloned.1.call-start
  104.0 0.0 copy-done.17
  104.0 0.0 copy-start.13
  104.0 1.1 copy-done.13
  105.1 1.1 copy-done.14
  106.2 1.1 copy-done.15
  107.3 96.9 %shard_map.145 = (bf16[704,2048]{1,0:T(8,128)(2,1)S(1)}, bf16[704,2048]{1,0:T(8,128)(2,1)S(1)}, bf16[2,352,2048]{2,1,0:T(8,128)(2,1)S(1)}) custom-call(f32[1,256]{1,0:T(1,128)S(1)} %bitcast.31, f32[704,256]{1,0:T(8,128)S(1)} %bitcast.28, f32[704,256]{1,0:T(8,128)S(1)} %bitcast.29, f32[352,512]{1,0:T(8,128)S(1)} %copy-done.15), custom_call_target="tpu_custom_call" | custom-call | flops 10000000000 | bytes 16777216 | tf_op jit(solution)/shard_map/pallas_call | solution.py:245
  204.2 0.0 copy-start.3
  204.2 1.6 copy-done.3
  205.8 1.6 copy-done.5
  207.4 1.6 copy-done.7
  209.0 5.1 %convert_add_fusion = (f32[512,2048]{1,0:T(8,128)}, f32[512]{0:T(512)S(1)}) fusion(bf16[512,2048]{1,0:T(8,128)(2,1)} %param.9, bf16[512,2048]{1,0:T(8,128)(2,1)} %all-reduce.2.cloned.1.call-done), kind=kLoop, calls=%fused_computation | loop fusion | flops 6290944 | bytes 8390656 | tf_op jit(solution)/shard_map/add | solution.py:315
  214.2 0.0 copy-done.8
  214.2 0.0 copy-done.19
  214.2 0.0 copy-done.20
  214.2 2.9 fusion.12
  217.1 9.2 %convolution_convert_fusion = bf16[512,2048]{1,0:T(8,128)(2,1)} fusion(bf16[704,2048]{1,0:T(8,128)(2,1)} %bitcast.22, bf16[704,2048]{1,0:T(8,128)(2,1)} %copy-done.5, f32[512,704]{0,1:T(8,128)} %fusion.12, f32[512]{0:T(512)S(1)} %add_rsqrt_fusion, bf16[512,2048]{1,0:T(8,128)(2,1)} %param.9, bf16[512,2048]{1,0:T(8,128)(2,1)} %all-reduce.2.cloned.1.call-done), kind=kOutput, calls=%fused_computation.7 | convolution fusion | flops 2962292736 | bytes 13502464 | tf_op jit(solution)/shard_map/dot_general | solution.py:294
  226.3 0.0 reduce-scatter.2.cloned.1.call-update
  226.3 51.9 %reduce-scatter.2.cloned.1.call-done = bf16[128,2048]{1,0:T(8,128)(2,1)} async-done(((bf16[512,2048]{1,0:T(8,128)(2,1)}), bf16[128,2048]{1,0:T(8,128)(2,1)}) %reduce-scatter.2.cloned.1.call-update) | async-done | bytes 524304 | tf_op jit(solution)/shard_map/reduce_scatter | solution.py:318
  278.2 2.3 add_convert_fusion
  280.5 3.9 %copy.23 = bf16[2048,704]{0,1:T(8,128)(2,1)} copy(bf16[2048,704]{0,1:T(8,128)(2,1)} %bitcast.21) | data formatting | bytes 5767168
  284.5 0.0 copy-done.1
  284.5 1.6 copy.24
  286.0 1.6 copy.25
  287.6 1.3 copy-done.9
  288.9 1.6 copy.26
  290.5 1.3 copy-done.6
  291.7 1.6 copy.27
  293.3 1.3 copy-done.4
  294.6 1.6 copy.28
  (17 shorter events, 0.0 us)
Async XLA Ops:
  7.2 201.8 %all-reduce.2.cloned.1.call-start = ((), (), s32[]{:S(2)}) async-start(), calls=%async_computation.1 | async-start | bytes 4194304 | tf_op jit(solution)/shard_map/psum | solution.py:313
  9.3 1.1 copy-start.10
  10.4 1.1 copy-start.11
  11.5 1.1 copy-start.12
  12.6 0.7 copy-start.16
  13.3 79.8 %copy-start.18 = (bf16[512,2048]{1,0:T(8,128)(2,1)S(1)}, bf16[512,2048]{1,0:T(8,128)(2,1)}, u32[]{:S(2)}) copy-start(bf16[512,2048]{1,0:T(8,128)(2,1)} %param.9) | copy-start | bytes 6291460
  93.1 3.0 copy-start
  93.1 3.0 copy-start.2
  96.1 7.8 %copy-start.17 = (f32[256]{0:T(256)S(1)}, f32[256]{0:T(256)}, u32[]{:S(2)}) copy-start(f32[256]{0:T(256)} %param.14) | copy-start | bytes 3076
  103.9 174.3 %reduce-scatter.2.cloned.1.call-start = ((), (), s32[]{:S(2)}) async-start(), calls=%async_computation.2 | async-start | bytes 2621440 | tf_op jit(solution)/shard_map/reduce_scatter | solution.py:318
  104.0 1.1 copy-start.13
  105.1 1.1 copy-start.14
  106.2 1.1 copy-start.15
  204.2 1.6 copy-start.3
  205.8 1.6 copy-start.5
  207.4 1.6 copy-start.7
  209.0 5.2 %copy-start.8 = (bf16[704,2048]{1,0:T(8,128)(2,1)S(1)}, bf16[704,2048]{1,0:T(8,128)(2,1)}, u32[]{:S(2)}) copy-start(bf16[704,2048]{1,0:T(8,128)(2,1)} %copy-done.7) | copy-start | bytes 8650756
  209.0 5.2 %copy-start.19 = (bf16[512,2048]{1,0:T(8,128)(2,1)S(1)}, bf16[512,2048]{1,0:T(8,128)(2,1)}, u32[]{:S(2)}) copy-start(bf16[512,2048]{1,0:T(8,128)(2,1)} %param.9) | copy-start | bytes 6291460
  209.0 5.2 %copy-start.20 = (bf16[512,2048]{1,0:T(8,128)(2,1)S(1)}, bf16[512,2048]{1,0:T(8,128)(2,1)}, u32[]{:S(2)}) copy-start(bf16[512,2048]{1,0:T(8,128)(2,1)} %all-reduce.2.cloned.1.call-done) | copy-start | bytes 6291460
  280.5 3.9 %copy-start.1 = (bf16[704,2048]{1,0:T(8,128)(2,1)S(1)}, bf16[704,2048]{1,0:T(8,128)(2,1)}, u32[]{:S(2)}) copy-start(bf16[704,2048]{1,0:T(8,128)(2,1)} %copy-done) | copy-start | bytes 8650756
  286.0 2.9 copy-start.9
  288.9 2.9 copy-start.6
  291.7 2.9 copy-start.4
Sparse Core Ops, SparseCore 0:
  104.0 82.8 all-reduce.1
  226.4 51.7 reduce-scatter.1

commit v2 on v1

--- a/solution.py
+++ b/solution.py
@@ -278,6 +278,399 @@
     )
 
 
+def fused_kernel(
+    n_gr,
+    n_fs,
+    n_tp,
+    prompt_ref,
+    gain_a,
+    gate_a,
+    up_a,
+    down_a,
+    gain_b,
+    gate_b,
+    up_b,
+    down_b,
+    gate_out_a,
+    up_out_a,
+    down_out_a,
+    gate_out_b,
+    up_out_b,
+    down_out_b,
+    mixed_ref,
+    down_own,
+    normed,
+    normed_all,
+    hidden,
+    parts,
+    parts_in,
+    stream,
+    line_send,
+    line_recv,
+    pair_send,
+    pair_recv,
+    part_send,
+    part_recv,
+    sum_send,
+    sum_recv,
+    row_send,
+    row_recv,
+):
+    g, f, t = lax.axis_index("gr"), lax.axis_index("fs"), lax.axis_index("tp")
+    per = n_gr * n_fs // n_tp
+    cols = down_a.shape[1]
+    width = gate_a.shape[1]
+    first = lax.rem(t * per, n_fs)
+    home = (t * per) // n_fs
+    row = g * n_fs + f
+    owner = row // per
+    slot = lax.rem(row, per)
+    outs = ((gate_out_a, up_out_a, down_out_a), (gate_out_b, up_out_b, down_out_b))
+
+    def place(ref, origin):
+        return ref.at[:, pl.ds(pl.multiple_of(origin * width, 128), width)]
+
+    for n, (gain, gate, up, down) in enumerate(
+        ((gain_a, gate_a, up_a, down_a), (gain_b, gate_b, up_b, down_b))
+    ):
+        place(outs[n][0], row)[...] = (gain[...] * gate[...]).astype(jnp.bfloat16)
+        place(outs[n][1], row)[...] = (gain[...] * up[...]).astype(jnp.bfloat16)
+        down_own[n] = down[...].astype(jnp.bfloat16)
+
+        @pl.when(owner == t)
+        def _(n=n, down=down):
+            outs[n][2][slot, :, pl.ds(pl.multiple_of(t * cols, 128), cols)] = down[...].astype(
+                jnp.bfloat16
+            )
+
+    barrier = pltpu.get_barrier_semaphore()
+    for dg in range(n_gr):
+        for dt in range(n_tp):
+            if dg or dt:
+                pl.semaphore_signal(
+                    barrier,
+                    inc=1,
+                    device_id=(lax.rem(g + dg, n_gr), f, lax.rem(t + dt, n_tp)),
+                    device_id_type=MESH,
+                )
+    for near in (lax.rem(f + 1, n_fs), lax.rem(f + n_fs - 1, n_fs)):
+        pl.semaphore_signal(barrier, inc=1, device_id=(g, near, t), device_id_type=MESH)
+    pl.semaphore_wait(barrier, n_gr * n_tp + 1)
+
+    def held(o):
+        return jnp.logical_and(o >= first, o < first + per)
+
+    def remote(src, dst, send, recv, to):
+        return pltpu.make_async_remote_copy(
+            src_ref=src,
+            dst_ref=dst,
+            send_sem=send,
+            recv_sem=recv,
+            device_id=to,
+            device_id_type=MESH,
+        )
+
+    def block(n, m, o):
+        if m < 2:
+            return place(outs[n][m], g * n_fs + o)
+        return outs[n][2].at[o - first]
+
+    def line(n, m, way, s):
+        step = 1 if way == 0 else -1
+        o = f - step * (s - 1)
+        sems = line_send.at[n, m, way, s], line_recv.at[n, m, way, s]
+        return remote(block(n, m, o), block(n, m, o), *sems, (g, f + step, t))
+
+    def sends(m, way, s):
+        step = 1 if way == 0 else -1
+        o = f - step * (s - 1)
+        fine = (f < n_fs - 1, o >= 0) if way == 0 else (f > 0, o <= n_fs - 1)
+        ok = jnp.logical_and(*fine)
+        return jnp.logical_and(ok, held(o)) if m == 2 else ok
+
+    def gets(m, way, s):
+        o = f - s if way == 0 else f + s
+        ok = o >= 0 if way == 0 else o <= n_fs - 1
+        return jnp.logical_and(ok, held(o)) if m == 2 else ok
+
+    def landed(n, m, way, s):
+        o = f - s if way == 0 else f + s
+        sems = line_send.at[n, m, way, s], line_recv.at[n, m, way, s]
+        return remote(block(n, m, o), block(n, m, o), *sems, (g, f, t))
+
+    def pair(n, m, dg, o):
+        spot = place(outs[n][m], g * n_fs + o)
+        sems = pair_send.at[n, m, dg, o], pair_recv.at[n, m, dg, o]
+        return remote(spot, spot, *sems, (lax.rem(g + dg, n_gr), f, t))
+
+    def pair_landed(n, m, dg, o):
+        src = lax.rem(g - dg + n_gr, n_gr)
+        spot = place(outs[n][m], src * n_fs + o)
+        sems = pair_send.at[n, m, dg, o], pair_recv.at[n, m, dg, o]
+        return remote(spot, spot, *sems, (src, f, t))
+
+    def part(n, dg):
+        return remote(
+            down_own.at[n],
+            outs[n][2].at[slot, :, pl.ds(pl.multiple_of(t * cols, 128), cols)],
+            part_send.at[n, dg],
+            part_recv.at[n, t],
+            (lax.rem(g + dg, n_gr), f, owner),
+        )
+
+    def part_landed(n, src):
+        return remote(
+            down_own.at[n],
+            outs[n][2].at[f - first, :, pl.ds(src * cols, cols)],
+            part_send.at[n, 0],
+            part_recv.at[n, src],
+            (home, f, src),
+        )
+
+    def start_own(n):
+        for m in range(2):
+            for way in range(2):
+
+                @pl.when(sends(m, way, 1))
+                def _(m=m, way=way):
+                    line(n, m, way, 1).start()
+
+            for dg in range(1, n_gr):
+                pair(n, m, dg, f).start()
+        for dg in range(n_gr):
+            if dg == 0:
+
+                @pl.when(owner != t)
+                def _():
+                    part(n, 0).start()
+
+            else:
+                part(n, dg).start()
+
+    def start_down(n):
+        @pl.when(held(f))
+        def _():
+            for src in range(n_tp):
+
+                @pl.when(jnp.logical_or(home != g, t != src))
+                def _(src=src):
+                    part_landed(n, src).wait_recv()
+
+        for way in range(2):
+
+            @pl.when(sends(2, way, 1))
+            def _(way=way):
+                line(n, 2, way, 1).start()
+
+    def forward(n, m, s):
+        for way in range(2):
+
+            @pl.when(gets(m, way, s))
+            def _(way=way):
+                landed(n, m, way, s).wait_recv()
+                if s < n_fs - 1:
+
+                    @pl.when(sends(m, way, s + 1))
+                    def _():
+                        line(n, m, way, s + 1).start()
+
+                if m < 2:
+                    o = f - s if way == 0 else f + s
+                    for dg in range(1, n_gr):
+                        pair(n, m, dg, o).start()
+
+    def pairs_in(n):
+        for m in range(2):
+            for dg in range(1, n_gr):
+                for o in range(n_fs):
+                    pair_landed(n, m, dg, o).wait_recv()
+
+    def drain(n):
+        for m in range(2):
+            for dg in range(1, n_gr):
+                for o in range(n_fs):
+                    pair(n, m, dg, o).wait_send()
+        for m in range(3):
+            for way in range(2):
+                for s in range(1, n_fs):
+
+                    @pl.when(sends(m, way, s))
+                    def _(m=m, way=way, s=s):
+                        line(n, m, way, s).wait_send()
+
+        for dg in range(n_gr):
+            if dg == 0:
+
+                @pl.when(owner != t)
+                def _():
+                    part(n, 0).wait_send()
+
+            else:
+                part(n, dg).wait_send()
+
+    owned, depth = prompt_ref.shape[1], prompt_ref.shape[2]
+    across = (((1,), (1,)), ((), ()))
+
+    def unit(rows):
+        return rows * lax.rsqrt(jnp.mean(rows * rows, axis=-1, keepdims=True) + 1e-06)
+
+    def hide(n, source):
+        @pl.loop(0, n_tp // 2)
+        def _(i):
+            rows = source[pl.ds(2 * i, 2)].reshape(2 * owned, depth)
+            gate = lax.dot_general(
+                rows, outs[n][0][...], across, preferred_element_type=jnp.float32
+            )
+            upper = lax.dot_general(
+                rows, outs[n][1][...], across, preferred_element_type=jnp.float32
+            )
+            units = (jax.nn.silu(gate) * upper).astype(jnp.bfloat16)
+            hidden[pl.ds(2 * i, 2)] = units.reshape(2, owned, units.shape[1])
+
+    def share(n, i):
+        to = lax.rem(t + 1 + i, n_tp)
+        return remote(
+            parts.at[n, to],
+            parts_in.at[n, i],
+            sum_send.at[n, i],
+            sum_recv.at[n, i],
+            (g, f, to),
+        )
+
+    def spread(n):
+        tall = outs[n][2].shape[1]
+
+        @pl.loop(0, n_tp)
+        def _(i):
+            to = lax.rem(t + 1 + i, n_tp)
+            units = hidden[to]
+            term = jnp.zeros((owned, depth), jnp.float32)
+            for k in range(per):
+                term += jnp.dot(
+                    units[:, k * tall : (k + 1) * tall],
+                    outs[n][2][k],
+                    preferred_element_type=jnp.float32,
+                )
+            parts[n, to] = term.astype(jnp.bfloat16)
+
+            @pl.when(i > 0)
+            def _():
+                share(n, i - 1).start()
+
+    def collect(n):
+        total = parts[n, t].astype(jnp.float32)
+        for i in range(n_tp - 1):
+            share(n, i).wait_recv()
+            total += parts_in[n, i].astype(jnp.float32)
+        return total
+
+    def give(i):
+        to = lax.rem(t + 1 + i, n_tp)
+        return remote(
+            normed_all.at[t], normed_all.at[t], row_send.at[i], row_recv.at[i], (g, f, to)
+        )
+
+    def given(i):
+        src = lax.rem(t - 1 - i + n_tp, n_tp)
+        return remote(
+            normed_all.at[src], normed_all.at[src], row_send.at[i], row_recv.at[i], (g, f, src)
+        )
+
+    start_own(0)
+
+    @pl.loop(0, n_tp)
+    def _(i):
+        normed[i] = unit(prompt_ref[i].astype(jnp.float32)).astype(jnp.bfloat16)
+
+    start_down(0)
+    for m in range(3):
+        forward(0, m, 1)
+    start_own(1)
+    for s in range(2, n_fs):
+        for m in range(3):
+            forward(0, m, s)
+    start_down(1)
+    pairs_in(0)
+    hide(0, normed)
+    for m in range(3):
+        forward(1, m, 1)
+    spread(0)
+    for s in range(2, n_fs - 1):
+        for m in range(3):
+            forward(1, m, s)
+    stream[...] = prompt_ref[t].astype(jnp.float32) + 0.5 * collect(0)
+    normed_all[t] = unit(stream[...]).astype(jnp.bfloat16)
+    for m in range(2):
+        forward(1, m, n_fs - 1)
+    for i in range(n_tp - 1):
+        give(i).start()
+    for i in range(n_tp - 1):
+        given(i).wait_recv()
+    pairs_in(1)
+    hide(1, normed_all)
+    forward(1, 2, n_fs - 1)
+    spread(1)
+    drain(0)
+    drain(1)
+    mixed_ref[...] = (stream[...] + 0.5 * collect(1)).astype(jnp.bfloat16)
+    for i in range(n_tp - 1):
+        give(i).wait_send()
+        share(0, i).wait_send()
+        share(1, i).wait_send()
+
+
+def fused(sizes, prompt, *weights):
+    n_gr, n_fs, n_tp = sizes
+    per = n_gr * n_fs // n_tp
+    tokens, depth = prompt.shape
+    owned = tokens // n_tp
+    rows, width = weights[1].shape
+    tall, cols = weights[3].shape
+    vmem = pl.BlockSpec(memory_space=pltpu.VMEM)
+    dma = pltpu.SemaphoreType.DMA
+    across = jax.ShapeDtypeStruct((width, n_gr * n_fs * rows), jnp.bfloat16)
+    down = jax.ShapeDtypeStruct((per, tall, n_tp * cols), jnp.bfloat16)
+    operands = [prompt.reshape(n_tp, owned, depth)]
+    for n in range(2):
+        gain, gate, up, tall_block = weights[4 * n : 4 * n + 4]
+        operands += [gain[None, :], gate.T, up.T, tall_block]
+    *served, mixed = pl.pallas_call(
+        functools.partial(fused_kernel, n_gr, n_fs, n_tp),
+        out_shape=(across, across, down) * 2
+        + (jax.ShapeDtypeStruct((owned, depth), jnp.bfloat16),),
+        in_specs=[vmem] * 9,
+        out_specs=(vmem,) * 7,
+        scratch_shapes=[
+            pltpu.VMEM((2, tall, cols), jnp.bfloat16),
+            pltpu.VMEM((n_tp, owned, depth), jnp.bfloat16),
+            pltpu.VMEM((n_tp, owned, depth), jnp.bfloat16),
+            pltpu.VMEM((n_tp, owned, width), jnp.bfloat16),
+            pltpu.VMEM((2, n_tp, owned, depth), jnp.bfloat16),
+            pltpu.VMEM((2, n_tp - 1, owned, depth), jnp.bfloat16),
+            pltpu.VMEM((owned, depth), jnp.float32),
+            dma((2, 3, 2, n_fs)),
+            dma((2, 3, 2, n_fs)),
+            dma((2, 2, n_gr, n_fs)),
+            dma((2, 2, n_gr, n_fs)),
+            dma((2, n_gr)),
+            dma((2, n_tp)),
+            dma((2, n_tp - 1)),
+            dma((2, n_tp - 1)),
+            dma((n_tp - 1,)),
+            dma((n_tp - 1,)),
+        ],
+        compiler_params=pltpu.CompilerParams(
+            collective_id=2, has_side_effects=True, vmem_limit_bytes=60 * 2**20
+        ),
+    )(*operands)
+    gate_a, up_a, down_a, gate_b, up_b, down_b = served
+
+    def flat(a):
+        return a.reshape(per * tall, n_tp * cols)
+
+    return (gate_a.T, up_a.T, flat(down_a), gate_b.T, up_b.T, flat(down_b), mixed)
+
+
 def normalize(rows):
     rows = rows.astype(jnp.float32)
     scale = lax.rsqrt(jnp.mean(rows * rows, axis=-1, keepdims=True) + 1e-06)
@@ -306,6 +699,19 @@
     up_second,
     down_second,
 ):
+    if gate_first.shape[0] % 128 == 0 and sizes[2] % 2 == 0:
+        return fused(
+            sizes,
+            prompt,
+            gain_first,
+            gate_first,
+            up_first,
+            down_first,
+            gain_second,
+            gate_second,
+            up_second,
+            down_second,
+        )
     gate_a, up_a, down_a = gather(sizes, 0, gain_first, gate_first, up_first, down_first)
     hidden_a = hidden_units(normalize(prompt), gate_a, up_a)
     term_a = rounded_term(hidden_a, down_a)

time: 305 us -> 247 us (0.81)
  Pallas kernels: 177 us -> 229 us
  waiting for transfers between devices: 51.9 us -> 0 us
  matrix products: 22.8 us -> 0 us
  between operations: 14.2 us -> 0.66 us
  local copies, waits for them, and re-layouts: 27.8 us -> 17.7 us
  other arithmetic: 9.54 us -> 0 us
    pallas_call x2 -> x1, Pallas kernels: 177 us -> 229 us  [fused(): pl.pallas_call(functools.partial(fused_kernel, n_gr, n_fs, n_tp), out_sha...]
    reduce_scatter x1 -> x0, waiting for transfers between devices: 51.9 us -> none  [shards(): lax.psum_scatter(rounded_term(hidden_b, down_b), 'tp', scatter_dimension=...]
    dot_general x4 -> x0, matrix products: 22.8 us -> none  [the longest x2 17 us: rounded_term(): jnp.dot(hidden, w_down, preferred_element_type=jnp.float32)]
    unnamed x48 -> x19, local copies, waits for them, and re-layouts: 27.8 us -> 17.7 us
    add x1 -> x0, other arithmetic: 5.14 us -> none  [shards(): stream = prompt.astype(jnp.float32) + 0.5 * branch_a]
  transfers between devices with their start and end apart: 2 -> 0, of which waited for: 1 -> 0; matrix products, arithmetic and copies ran while one was open for 0% -> 0% of each run, Pallas kernels for 32% -> 0%
where the time goes in v2:
time: 247 us
  Pallas kernels  229 us (93%)
  local copies, waits for them, and re-layouts  17.7 us (7%)
    pallas_call x1, Pallas kernels, fused(): pl.pallas_call(functools.partial(fused_kernel, n_gr, n_fs, n_tp), out_sha...  229 us
    unnamed x19, local copies, waits for them, and re-layouts  17.7 us

profile of v2, /device:TPU:25, one launch (start us, length us, event | category | flops | bytes accessed | tf_op | source)
XLA Modules:
  0.0 247.0 jit_solution(6730734963358884879)
XLA Ops:
  0.6 228.6 %shard_map.144 = (bf16[704,2048]{1,0:T(8,128)(2,1)}, bf16[704,2048]{1,0:T(8,128)(2,1)}, bf16[2,352,2048]{2,1,0:T(8,128)(2,1)}, bf16[704,2048]{1,0:T(8,128)(2,1)}...) custom-call(bf16[4,128,2048]{2,1,0:T(8,128)(2,1)} %bitcast.19, ...), custom_call_target="tpu_custom_call" | custom-call | tf_op jit(solution)/shard_map/pallas_call | solution.py:637
  229.3 0.0 copy-start.4
  229.3 3.9 %copy.23 = bf16[2048,704]{0,1:T(8,128)(2,1)} copy(bf16[2048,704]{0,1:T(8,128)(2,1)} %bitcast.18) | data formatting | bytes 5767168
  233.2 0.0 copy-done.4
  233.2 0.0 copy-start.3
  233.2 1.6 copy.24
  234.8 1.3 copy-done.3
  236.0 0.0 copy-start.2
  236.0 1.6 copy.25
  237.6 1.3 copy-done.2
  238.9 0.0 copy-start.1
  238.9 1.6 copy.26
  240.5 1.3 copy-done.1
  241.8 0.0 copy-start
  241.8 1.6 copy.27
  243.3 1.3 copy-done
  244.6 0.0 copy-start.5
  244.6 1.6 copy.28
  246.2 0.0 copy-done.5
  246.2 0.8 copy.29
Async XLA Ops:
  229.3 3.9 %copy-start.4 = (bf16[704,2048]{1,0:T(8,128)(2,1)S(1)}, bf16[704,2048]{1,0:T(8,128)(2,1)}, u32[]{:S(2)}) copy-start(bf16[704,2048]{1,0:T(8,128)(2,1)} %get-tuple-element.15) | copy-start | bytes 8650756
  233.2 2.9 %copy-start.3 = (bf16[2,352,2048]{2,1,0:T(8,128)(2,1)S(1)}, bf16[2,352,2048]{2,1,0:T(8,128)(2,1)}, u32[]{:S(2)}) copy-start(bf16[2,352,2048]{2,1,0:T(8,128)(2,1)} %get-tuple-element.16) | copy-start | bytes 8650756
  236.0 2.9 %copy-start.2 = (bf16[704,2048]{1,0:T(8,128)(2,1)S(1)}, bf16[704,2048]{1,0:T(8,128)(2,1)}, u32[]{:S(2)}) copy-start(bf16[704,2048]{1,0:T(8,128)(2,1)} %get-tuple-element.17) | copy-start | bytes 8650756
  238.9 2.9 %copy-start.1 = (bf16[704,2048]{1,0:T(8,128)(2,1)S(1)}, bf16[704,2048]{1,0:T(8,128)(2,1)}, u32[]{:S(2)}) copy-start(bf16[704,2048]{1,0:T(8,128)(2,1)} %get-tuple-element.18) | copy-start | bytes 8650756
  241.8 2.9 %copy-start = (bf16[2,352,2048]{2,1,0:T(8,128)(2,1)S(1)}, bf16[2,352,2048]{2,1,0:T(8,128)(2,1)}, u32[]{:S(2)}) copy-start(bf16[2,352,2048]{2,1,0:T(8,128)(2,1)} %get-tuple-element.19) | copy-start | bytes 8650756
  244.6 1.6 copy-start.5

commit v3 on v2

--- a/solution.py
+++ b/solution.py
@@ -303,7 +303,10 @@
     normed_all,
     hidden,
     parts,
+    mate_in,
+    sums,
     parts_in,
+    kept,
     stream,
     line_send,
     line_recv,
@@ -311,6 +314,8 @@
     pair_recv,
     part_send,
     part_recv,
+    mate_send,
+    mate_recv,
     sum_send,
     sum_recv,
     row_send,
@@ -325,7 +330,12 @@
     row = g * n_fs + f
     owner = row // per
     slot = lax.rem(row, per)
+    half = n_tp * cols // n_gr
+    lane = t * n_gr // n_tp
     outs = ((gate_out_a, up_out_a, down_out_a), (gate_out_b, up_out_b, down_out_b))
+
+    def halved(n):
+        return n == 1
 
     def place(ref, origin):
         return ref.at[:, pl.ds(pl.multiple_of(origin * width, 128), width)]
@@ -337,7 +347,7 @@
         place(outs[n][1], row)[...] = (gain[...] * up[...]).astype(jnp.bfloat16)
         down_own[n] = down[...].astype(jnp.bfloat16)
 
-        @pl.when(owner == t)
+        @pl.when(jnp.logical_and(owner == t, lane == g) if halved(n) else owner == t)
         def _(n=n, down=down):
             outs[n][2][slot, :, pl.ds(pl.multiple_of(t * cols, 128), cols)] = down[...].astype(
                 jnp.bfloat16
@@ -373,7 +383,12 @@
     def block(n, m, o):
         if m < 2:
             return place(outs[n][m], g * n_fs + o)
+        if halved(n):
+            return share_of(n, o, g)
         return outs[n][2].at[o - first]
+
+    def share_of(n, o, column):
+        return outs[n][2].at[o - first, :, pl.ds(pl.multiple_of(column * half, 128), half)]
 
     def line(n, m, way, s):
         step = 1 if way == 0 else -1
@@ -399,13 +414,13 @@
         return remote(block(n, m, o), block(n, m, o), *sems, (g, f, t))
 
     def pair(n, m, dg, o):
-        spot = place(outs[n][m], g * n_fs + o)
+        spot = share_of(n, o, g) if m == 2 else place(outs[n][m], g * n_fs + o)
         sems = pair_send.at[n, m, dg, o], pair_recv.at[n, m, dg, o]
         return remote(spot, spot, *sems, (lax.rem(g + dg, n_gr), f, t))
 
     def pair_landed(n, m, dg, o):
         src = lax.rem(g - dg + n_gr, n_gr)
-        spot = place(outs[n][m], src * n_fs + o)
+        spot = share_of(n, o, src) if m == 2 else place(outs[n][m], src * n_fs + o)
         sems = pair_send.at[n, m, dg, o], pair_recv.at[n, m, dg, o]
         return remote(spot, spot, *sems, (src, f, t))
 
@@ -415,7 +430,7 @@
             outs[n][2].at[slot, :, pl.ds(pl.multiple_of(t * cols, 128), cols)],
             part_send.at[n, dg],
             part_recv.at[n, t],
-            (lax.rem(g + dg, n_gr), f, owner),
+            (lane if halved(n) else lax.rem(g + dg, n_gr), f, owner),
         )
 
     def part_landed(n, src):
@@ -438,7 +453,14 @@
             for dg in range(1, n_gr):
                 pair(n, m, dg, f).start()
         for dg in range(n_gr):
-            if dg == 0:
+            if halved(n):
+                if dg == 0:
+
+                    @pl.when(jnp.logical_or(owner != t, lane != g))
+                    def _():
+                        part(n, 0).start()
+
+            elif dg == 0:
 
                 @pl.when(owner != t)
                 def _():
@@ -452,9 +474,17 @@
         def _():
             for src in range(n_tp):
 
-                @pl.when(jnp.logical_or(home != g, t != src))
+                away = jnp.logical_or(home != g, t != src)
+                if halved(n):
+                    away = jnp.logical_and(away, g == src * n_gr // n_tp)
+
+                @pl.when(away)
                 def _(src=src):
                     part_landed(n, src).wait_recv()
+
+            if halved(n):
+                for dg in range(1, n_gr):
+                    pair(n, 2, dg, f).start()
 
         for way in range(2):
 
@@ -474,7 +504,7 @@
                     def _():
                         line(n, m, way, s + 1).start()
 
-                if m < 2:
+                if m < 2 or halved(n):
                     o = f - s if way == 0 else f + s
                     for dg in range(1, n_gr):
                         pair(n, m, dg, o).start()
@@ -485,7 +515,17 @@
                 for o in range(n_fs):
                     pair_landed(n, m, dg, o).wait_recv()
 
+    def halves(n, act):
+        for dg in range(1, n_gr):
+            for o in range(n_fs):
+
+                @pl.when(held(o))
+                def _(dg=dg, o=o):
+                    act(n, 2, dg, o)
+
     def drain(n):
+        if halved(n):
+            halves(n, lambda *at: pair(*at).wait_send())
         for m in range(2):
             for dg in range(1, n_gr):
                 for o in range(n_fs):
@@ -499,7 +539,14 @@
                         line(n, m, way, s).wait_send()
 
         for dg in range(n_gr):
-            if dg == 0:
+            if halved(n):
+                if dg == 0:
+
+                    @pl.when(jnp.logical_or(owner != t, lane != g))
+                    def _():
+                        part(n, 0).wait_send()
+
+            elif dg == 0:
 
                 @pl.when(owner != t)
                 def _():
@@ -527,41 +574,63 @@
             units = (jax.nn.silu(gate) * upper).astype(jnp.bfloat16)
             hidden[pl.ds(2 * i, 2)] = units.reshape(2, owned, units.shape[1])
 
-    def share(n, i):
-        to = lax.rem(t + 1 + i, n_tp)
+    pairs = n_tp // 2
+    seat, core = t // 2, lax.rem(t, 2)
+
+    def at_seat(j):
+        return 2 * lax.rem(seat + 1 + j, pairs)
+
+    def mate(n, j):
         return remote(
-            parts.at[n, to],
-            parts_in.at[n, i],
-            sum_send.at[n, i],
-            sum_recv.at[n, i],
-            (g, f, to),
-        )
+            parts.at[n, j],
+            mate_in.at[n, j],
+            mate_send.at[n, j],
+            mate_recv.at[n, j],
+            (g, f, t + 1 - 2 * core),
+        )
+
+    def share(n, j):
+        return remote(
+            sums.at[n, j],
+            parts_in.at[n, j],
+            sum_send.at[n, j],
+            sum_recv.at[n, j],
+            (g, f, at_seat(j) + core),
+        )
+
+    def term(n, units):
+        tall = outs[n][2].shape[1]
+        total = jnp.zeros((owned, depth), jnp.float32)
+        for k in range(per):
+            total += jnp.dot(
+                units[:, k * tall : (k + 1) * tall],
+                outs[n][2][k],
+                preferred_element_type=jnp.float32,
+            )
+        return total.astype(jnp.bfloat16)
 
     def spread(n):
-        tall = outs[n][2].shape[1]
-
-        @pl.loop(0, n_tp)
-        def _(i):
-            to = lax.rem(t + 1 + i, n_tp)
-            units = hidden[to]
-            term = jnp.zeros((owned, depth), jnp.float32)
-            for k in range(per):
-                term += jnp.dot(
-                    units[:, k * tall : (k + 1) * tall],
-                    outs[n][2][k],
-                    preferred_element_type=jnp.float32,
-                )
-            parts[n, to] = term.astype(jnp.bfloat16)
-
-            @pl.when(i > 0)
-            def _():
-                share(n, i - 1).start()
+        for j in range(pairs):
+            parts[n, j] = term(n, hidden[at_seat(j) + 1 - core])
+            if j > 0:
+                mate(n, j - 1).start()
+        for j in range(pairs):
+            mine = term(n, hidden[at_seat(j) + core]).astype(jnp.float32)
+            if j == 0:
+                mate(n, pairs - 1).start()
+            mate(n, j).wait_recv()
+            both = mine + mate_in[n, j].astype(jnp.float32)
+            if j < pairs - 1:
+                sums[n, j] = both.astype(jnp.bfloat16)
+                share(n, j).start()
+            else:
+                kept[...] = both
 
     def collect(n):
-        total = parts[n, t].astype(jnp.float32)
-        for i in range(n_tp - 1):
-            share(n, i).wait_recv()
-            total += parts_in[n, i].astype(jnp.float32)
+        total = kept[...]
+        for j in range(pairs - 1):
+            share(n, j).wait_recv()
+            total += parts_in[n, j].astype(jnp.float32)
         return total
 
     def give(i):
@@ -609,14 +678,18 @@
     pairs_in(1)
     hide(1, normed_all)
     forward(1, 2, n_fs - 1)
+    halves(1, lambda *at: pair_landed(*at).wait_recv())
     spread(1)
     drain(0)
     drain(1)
     mixed_ref[...] = (stream[...] + 0.5 * collect(1)).astype(jnp.bfloat16)
     for i in range(n_tp - 1):
         give(i).wait_send()
-        share(0, i).wait_send()
-        share(1, i).wait_send()
+    for n in range(2):
+        for j in range(pairs):
+            mate(n, j).wait_send()
+            if j < pairs - 1:
+                share(n, j).wait_send()
 
 
 def fused(sizes, prompt, *weights):
@@ -628,8 +701,8 @@
     tall, cols = weights[3].shape
     vmem = pl.BlockSpec(memory_space=pltpu.VMEM)
     dma = pltpu.SemaphoreType.DMA
-    across = jax.ShapeDtypeStruct((width, n_gr * n_fs * rows), jnp.bfloat16)
-    down = jax.ShapeDtypeStruct((per, tall, n_tp * cols), jnp.bfloat16)
+    across = pltpu.VMEM((width, n_gr * n_fs * rows), jnp.bfloat16)
+    down = pltpu.VMEM((per, tall, n_tp * cols), jnp.bfloat16)
     operands = [prompt.reshape(n_tp, owned, depth)]
     for n in range(2):
         gain, gate, up, tall_block = weights[4 * n : 4 * n + 4]
@@ -645,22 +718,27 @@
             pltpu.VMEM((n_tp, owned, depth), jnp.bfloat16),
             pltpu.VMEM((n_tp, owned, depth), jnp.bfloat16),
             pltpu.VMEM((n_tp, owned, width), jnp.bfloat16),
-            pltpu.VMEM((2, n_tp, owned, depth), jnp.bfloat16),
-            pltpu.VMEM((2, n_tp - 1, owned, depth), jnp.bfloat16),
+            pltpu.VMEM((2, n_tp // 2, owned, depth), jnp.bfloat16),
+            pltpu.VMEM((2, n_tp // 2, owned, depth), jnp.bfloat16),
+            pltpu.VMEM((2, n_tp // 2, owned, depth), jnp.bfloat16),
+            pltpu.VMEM((2, n_tp // 2, owned, depth), jnp.bfloat16),
+            pltpu.VMEM((owned, depth), jnp.float32),
             pltpu.VMEM((owned, depth), jnp.float32),
             dma((2, 3, 2, n_fs)),
             dma((2, 3, 2, n_fs)),
-            dma((2, 2, n_gr, n_fs)),
-            dma((2, 2, n_gr, n_fs)),
+            dma((2, 3, n_gr, n_fs)),
+            dma((2, 3, n_gr, n_fs)),
             dma((2, n_gr)),
             dma((2, n_tp)),
-            dma((2, n_tp - 1)),
-            dma((2, n_tp - 1)),
+            dma((2, n_tp // 2)),
+            dma((2, n_tp // 2)),
+            dma((2, n_tp // 2)),
+            dma((2, n_tp // 2)),
             dma((n_tp - 1,)),
             dma((n_tp - 1,)),
         ],
         compiler_params=pltpu.CompilerParams(
-            collective_id=2, has_side_effects=True, vmem_limit_bytes=60 * 2**20
+            collective_id=2, has_side_effects=True, vmem_limit_bytes=40 * 2**20
         ),
     )(*operands)
     gate_a, up_a, down_a, gate_b, up_b, down_b = served

time: 247 us -> 238 us (0.964)
  local copies, waits for them, and re-layouts: 17.7 us -> 10.3 us
    unnamed x19 -> x9, local copies, waits for them, and re-layouts: 17.7 us -> 10.3 us
where the time goes in v3:
time: 238 us
  Pallas kernels  227 us (95%)
  local copies, waits for them, and re-layouts  10.3 us (4%)
    pallas_call x1, Pallas kernels, fused(): pl.pallas_call(functools.partial(fused_kernel, n_gr, n_fs, n_tp), out_sha...  227 us
    unnamed x9, local copies, waits for them, and re-layouts  10.3 us

profile of v3, /device:TPU:25, one launch (start us, length us, event | category | flops | bytes accessed | tf_op | source)
XLA Modules:
  0.0 237.5 jit_solution(16329368512831116397)
XLA Ops:
  0.6 226.6 %shard_map.144 = (bf16[704,2048]{1,0:T(8,128)(2,1)S(1)}, bf16[704,2048]{1,0:T(8,128)(2,1)S(1)}, bf16[2,352,2048]{2,1,0:T(8,128)(2,1)S(1)}, bf16[704,2048]{1,0:T(...) custom-call(bf16[4,128,2048]{2,1,0:T(8,128)(2,1)} %bitcast.19, ...), custom_call_target="tpu_custom_call" | custom-call | tf_op jit(solution)/shard_map/pallas_call | solution.py:710
  227.2 1.6 copy.23
  228.8 1.6 copy.24
  230.4 1.6 copy.25
  232.0 1.6 copy.26
  233.6 1.6 copy.27
  235.1 0.0 copy-start
  235.1 1.6 copy.28
  236.7 0.0 copy-done
  236.7 0.8 copy.29
Async XLA Ops:
  235.1 1.6 copy-start

commit v4 on v3

--- a/solution.py
+++ b/solution.py
@@ -659,10 +659,10 @@
         for m in range(3):
             forward(0, m, s)
     start_down(1)
+    for m in range(3):
+        forward(1, m, 1)
     pairs_in(0)
     hide(0, normed)
-    for m in range(3):
-        forward(1, m, 1)
     spread(0)
     for s in range(2, n_fs - 1):
         for m in range(3):
@@ -676,8 +676,8 @@
     for i in range(n_tp - 1):
         given(i).wait_recv()
     pairs_in(1)
+    forward(1, 2, n_fs - 1)
     hide(1, normed_all)
-    forward(1, 2, n_fs - 1)
     halves(1, lambda *at: pair_landed(*at).wait_recv())
     spread(1)
     drain(0)

time: 238 us -> 231 us (0.971)
  Pallas kernels: 227 us -> 219 us
    pallas_call x1, Pallas kernels: 227 us -> 219 us  [fused(): pl.pallas_call(functools.partial(fused_kernel, n_gr, n_fs, n_tp), out_sha...]
where the time goes in v4:
time: 231 us; the launch traced here: 230 us
  Pallas kernels  219 us (95%)
  local copies, waits for them, and re-layouts  10.3 us (4%)
    pallas_call x1, Pallas kernels, fused(): pl.pallas_call(functools.partial(fused_kernel, n_gr, n_fs, n_tp), out_sha...  219 us
    unnamed x9, local copies, waits for them, and re-layouts  10.3 us

profile of v4, /device:TPU:25, one launch (start us, length us, event | category | flops | bytes accessed | tf_op | source)
XLA Modules:
  0.0 230.2 jit_solution(1275434808466390095)
XLA Ops:
  0.6 219.3 %shard_map.144 = (bf16[704,2048]{1,0:T(8,128)(2,1)S(1)}, bf16[704,2048]{1,0:T(8,128)(2,1)S(1)}, bf16[2,352,2048]{2,1,0:T(8,128)(2,1)S(1)}, bf16[704,2048]{1,0:T(...) custom-call(bf16[4,128,2048]{2,1,0:T(8,128)(2,1)} %bitcast.19, ...), custom_call_target="tpu_custom_call" | custom-call | tf_op jit(solution)/shard_map/pallas_call | solution.py:710
  219.9 1.6 copy.23
  221.5 1.6 copy.24
  223.1 1.6 copy.25
  224.6 1.6 copy.26
  226.2 1.6 copy.27
  227.8 0.0 copy-start
  227.8 1.6 copy.28
  229.4 0.0 copy-done
  229.4 0.8 copy.29
Async XLA Ops:
  227.8 1.6 copy-start
